TPU v7x, 32 devices: a whole 2x2x4 slice. The times are simulated.
32 devices in a mesh: sp: 4 (over z), dp: 8 (over y, x, core).
Axes of the slice: x: 2, y: 2, z: 4, core: 2. Of those that a mesh axis runs over, the one named last changes fastest.
Arguments:
- inputs: bfloat16 [8, 544, 2048], P('dp', 'sp'), may hold values from -6 to 6
- query_vectors: bfloat16 [8, 544, 1024], P('dp', 'sp'), may hold values from -6 to 6
- key_vectors: bfloat16 [8, 544, 1024], P('dp', 'sp'), may hold values from -6 to 6
- value_vectors: bfloat16 [8, 544, 1024], P('dp', 'sp'), may hold values from -6 to 6
- cotangent: bfloat16 [8, 544, 1024], P('dp', 'sp'), may hold values from -6 to 6
- gate_prefix: float32 [8, 16, 544], P('dp', 'sp'), may hold values from -544 to 0, as said below
- value_weight: bfloat16 [2048, 1024], P('sp', 'dp'), may hold values from -0.125 to 0.125
Outputs:
- query_grad: bfloat16 [8, 544, 1024], P('dp', 'sp')
- key_grad: bfloat16 [8, 544, 1024], P('dp', 'sp')
- input_grad: bfloat16 [8, 544, 2048], P('dp', 'sp')
- weight_grad: float32 [2048, 1024], P('sp', 'dp')
Inputs may be any that keep to these rules, and one draw needn't show every extreme that they name: `gate_prefix`: non-increasing along the positions of each sequence and head.
All inputs are finite; a program needn't handle non-finite values.
Results may differ from a plain program's by a relative error of at most 0.015.
Values may be sent and summed in bfloat16 or wider, within the bound.
A program may use at most 128 MiB of HBM per device.

v0:
```python
import jax
import jax.numpy as jnp
from jax import lax
from jax.sharding import PartitionSpec as P

HEAD_DIM = 64


def attention_backward(query_heads, key_heads, value_heads, grad_heads, prefix):
    length = query_heads.shape[0]
    score_scale = HEAD_DIM ** (-0.5)
    block_count = max(1, length // 512)
    block_rows = length // block_count
    key_accum = jnp.zeros(key_heads.shape, jnp.float32)
    value_accum = jnp.zeros(key_heads.shape, jnp.float32)
    query_parts = []
    for block_index in range(block_count):
        first_row = block_index * block_rows
        last_row = first_row + block_rows
        query_rows = query_heads[first_row:last_row]
        key_rows = key_heads[:last_row]
        grad_rows = grad_heads[first_row:last_row]
        scores = (
            jnp.einsum("qhd,khd->hqk", query_rows, key_rows, preferred_element_type=jnp.float32)
            * score_scale
        )
        scores = scores + prefix[:, first_row:last_row, None] - prefix[:, None, :last_row]
        causal = jnp.arange(last_row)[None, :] <= (first_row + jnp.arange(block_rows))[:, None]
        scores = jnp.where(causal[None], scores, -jnp.inf)
        row_peak = jnp.max(scores, axis=-1, keepdims=True)
        raised_scores = jnp.exp(scores - row_peak)
        softmax_rows = raised_scores / jnp.sum(raised_scores, axis=-1, keepdims=True)
        softmax_low = softmax_rows.astype(jnp.bfloat16)
        value_accum = value_accum.at[:last_row].add(
            jnp.einsum("hqk,qhd->khd", softmax_low, grad_rows, preferred_element_type=jnp.float32)
        )
        softmax_grad = jnp.einsum(
            "qhd,khd->hqk", grad_rows, value_heads[:last_row], preferred_element_type=jnp.float32
        )
        row_term = jnp.sum(softmax_rows * softmax_grad, axis=-1, keepdims=True)
        score_low = (softmax_rows * (softmax_grad - row_term)).astype(jnp.bfloat16)
        query_parts.append(
            (
                jnp.einsum("hqk,khd->qhd", score_low, key_rows, preferred_element_type=jnp.float32)
                * score_scale
            ).astype(jnp.bfloat16)
        )
        key_accum = key_accum.at[:last_row].add(
            jnp.einsum("hqk,qhd->khd", score_low, query_rows, preferred_element_type=jnp.float32)
        )
    query_grad = jnp.concatenate(query_parts, axis=0)
    key_grad = (key_accum * score_scale).astype(jnp.bfloat16)
    return (query_grad, key_grad, value_accum.astype(jnp.bfloat16))


def shards(inputs, query_vectors, key_vectors, value_vectors, cotangent, gate_prefix, value_weight):
    query_seq, key_seq, value_seq, grad_seq, input_cols = (
        lax.all_to_all(query_vectors[0], "sp", split_axis=1, concat_axis=0, tiled=True),
        lax.all_to_all(key_vectors[0], "sp", split_axis=1, concat_axis=0, tiled=True),
        lax.all_to_all(value_vectors[0], "sp", split_axis=1, concat_axis=0, tiled=True),
        lax.all_to_all(cotangent[0], "sp", split_axis=1, concat_axis=0, tiled=True),
        lax.all_to_all(inputs[0], "sp", split_axis=1, concat_axis=0, tiled=True),
    )
    length = query_seq.shape[0]
    local_width = query_seq.shape[1]
    head_shape = (length, local_width // HEAD_DIM, HEAD_DIM)
    query_heads, key_heads, value_heads = attention_backward(
        query_seq.reshape(head_shape),
        key_seq.reshape(head_shape),
        value_seq.reshape(head_shape),
        grad_seq.reshape(head_shape),
        gate_prefix[0],
    )
    query_flat = query_heads.reshape(length, local_width)
    key_flat = key_heads.reshape(length, local_width)
    value_flat = value_heads.reshape(length, local_width)
    value_all = lax.all_gather(value_flat, "sp", axis=1, tiled=True)
    weight_block = lax.all_gather(value_weight, "dp", axis=1, tiled=True)
    weight_rows = lax.psum_scatter(
        lax.dot_general(
            value_all, input_cols, (((0,), (0,)), ((), ())), preferred_element_type=jnp.float32
        ).astype(jnp.bfloat16),
        "dp",
        scatter_dimension=0,
        tiled=True,
    ).astype(jnp.float32)
    weight_grad = weight_rows.T
    query_back, key_back = (
        lax.all_to_all(query_flat, "sp", split_axis=0, concat_axis=1, tiled=True),
        lax.all_to_all(key_flat, "sp", split_axis=0, concat_axis=1, tiled=True),
    )
    column_grad = lax.dot_general(
        value_all, weight_block, (((1,), (1,)), ((), ())), preferred_element_type=jnp.float32
    ).astype(jnp.bfloat16)
    input_grad = lax.all_to_all(column_grad, "sp", split_axis=0, concat_axis=1, tiled=True)
    return (query_back[None], key_back[None], input_grad[None], weight_grad)


def solution(mesh):
    in_specs = (
        P("dp", "sp", None),
        P("dp", "sp", None),
        P("dp", "sp", None),
        P("dp", "sp", None),
        P("dp", "sp", None),
        P("dp", "sp", None),
        P("sp", "dp"),
    )
    out_specs = (P("dp", "sp", None), P("dp", "sp", None), P("dp", "sp", None), P("sp", "dp"))
    return jax.shard_map(shards, mesh=mesh, in_specs=in_specs, out_specs=out_specs, check_vma=False)
```

profile of v0, /device:TPU:0, one launch (start us, length us, event | category | flops | bytes accessed | tf_op | source)
XLA Modules:
  0.0 171.9 jit_solution(9864498030525884451)
XLA Ops:
  9.1 6.3 %all-to-all-start = ((bf16[136,4,256]{2,0,1:T(8,128)(2,1)}), bf16[136,4,256]{2,0,1:T(8,128)(2,1)S(1)}, u32[]{:S(2)}, u32[]{:S(2)}) async-start(bf16[136,4,256]{2,0,1:T(8,128)(2,1)} %copy.61), calls=%async_computation | async-start | bytes 557056 | tf_op jit(solution)/shard_map/all_to_all | solution.py:58
  17.3 7.4 %all-to-all-done = bf16[136,4,256]{2,0,1:T(8,128)(2,1)S(1)} async-done(((bf16[136,4,256]{2,0,1:T(8,128)(2,1)}), bf16[136,4,256]{2,0,1:T(8,128)(2,1)S(1)}, u32[]{:S(2)}, u32[]{:S(2)}) %all-to-all-start) | async-done | bytes 278560 | tf_op jit(solution)/shard_map/all_to_all | solution.py:58
  24.7 3.5 %all-to-all-start.1 = ((bf16[136,4,256]{2,0,1:T(8,128)(2,1)}), bf16[136,4,256]{2,0,1:T(8,128)(2,1)S(1)}, u32[]{:S(2)}, u32[]{:S(2)}) async-start(bf16[136,4,256]{2,0,1:T(8,128)(2,1)} %copy.62), calls=%async_computation.1 | async-start | bytes 557056 | tf_op jit(solution)/shard_map/all_to_all | solution.py:59
  30.1 5.2 %all-to-all-done.1 = bf16[136,4,256]{2,0,1:T(8,128)(2,1)S(1)} async-done(((bf16[136,4,256]{2,0,1:T(8,128)(2,1)}), bf16[136,4,256]{2,0,1:T(8,128)(2,1)S(1)}, u32[]{:S(2)}, u32[]{:S(2)}) %all-to-all-start.1) | async-done | bytes 278560 | tf_op jit(solution)/shard_map/all_to_all | solution.py:59
  35.3 3.5 %all-to-all-start.2 = ((bf16[136,4,256]{2,0,1:T(8,128)(2,1)}), bf16[136,4,256]{2,0,1:T(8,128)(2,1)S(1)}, u32[]{:S(2)}, u32[]{:S(2)}) async-start(bf16[136,4,256]{2,0,1:T(8,128)(2,1)} %copy.65), calls=%async_computation.2 | async-start | bytes 557056 | tf_op jit(solution)/shard_map/all_to_all | solution.py:61
  40.2 5.4 %all-to-all-done.2 = bf16[136,4,256]{2,0,1:T(8,128)(2,1)S(1)} async-done(((bf16[136,4,256]{2,0,1:T(8,128)(2,1)}), bf16[136,4,256]{2,0,1:T(8,128)(2,1)S(1)}, u32[]{:S(2)}, u32[]{:S(2)}) %all-to-all-start.2) | async-done | bytes 278560 | tf_op jit(solution)/shard_map/all_to_all | solution.py:61
  46.3 4.4 %fusion.22 = (f32[4,544]{1,0:T(4,128)S(1)}, f32[4,544,544]{1,2,0:T(8,128)}) fusion(f32[4,544]{1,0:T(4,128)S(1)} %bitcast.46, pred[544,544]{0,1:T(8,128)(4,1)S(1)} %iota_compare_fusion, bf16[544,4,64]{0,2,1:T(8,128)(2,1)S(1)} %copy.63, bf16[544,4,64]{0,2,1:T(8,128)(2,1)S(1)} %copy.64), kind=kOutput, calls=%fused_computation.30 | convolution fusion | flops 158622240 | bytes 5605376 | tf_op jit(solution)/shard_map/sub | solution.py:31
  50.6 3.8 %fusion.11 = bf16[4,544,64]{1,2,0:T(8,128)(2,1)} fusion(bf16[544,4,64]{0,2,1:T(8,128)(2,1)S(1)} %copy.67, f32[4,544]{1,0:T(4,128)S(1)} %get-tuple-element.60, f32[4,544]{1,0:T(4,128)S(1)} %bitcast.47, pred[544,544]{0,1:T(8,128)(4,1)S(1)} %iota_compare_fusion, bf16[544,4,64]{0,2,1:T(8,128)(2,1)S(1)} %copy.63, bf16[544,4,64]{0,2,1:T(8,128)(2,1)S(1)} %copy.64), kind=kOutput, calls=%fused_computation.21 | convolution fusion | flops 311466656 | bytes 1427456 | tf_op jit(solution)/shard_map/hqk,qhd->khd/dot_general | solution.py:35
  55.4 3.5 %all-to-all-start.3 = ((bf16[136,4,256]{2,0,1:T(8,128)(2,1)}), bf16[136,4,256]{2,0,1:T(8,128)(2,1)S(1)}, u32[]{:S(2)}, u32[]{:S(2)}) async-start(bf16[136,4,256]{2,0,1:T(8,128)(2,1)} %copy.66), calls=%async_computation.3 | async-start | bytes 557056 | tf_op jit(solution)/shard_map/all_to_all | solution.py:60
  61.0 5.0 %all-to-all-done.3 = bf16[136,4,256]{2,0,1:T(8,128)(2,1)S(1)} async-done(((bf16[136,4,256]{2,0,1:T(8,128)(2,1)}), bf16[136,4,256]{2,0,1:T(8,128)(2,1)S(1)}, u32[]{:S(2)}, u32[]{:S(2)}) %all-to-all-start.3) | async-done | bytes 278560 | tf_op jit(solution)/shard_map/all_to_all | solution.py:60
  65.9 10.5 %all-to-all-start.7 = ((bf16[136,4,512]{2,0,1:T(8,128)(2,1)}), bf16[136,4,512]{2,0,1:T(8,128)(2,1)}, u32[]{:S(2)}, u32[]{:S(2)}) async-start(bf16[136,4,512]{2,0,1:T(8,128)(2,1)} %copy.80), calls=%async_computation.7 | async-start | bytes 1114112 | tf_op jit(solution)/shard_map/all_to_all | solution.py:62
  76.7 3.5 %multiply_reduce_fusion = (f32[4,544]{1,0:T(4,128)S(1)}, f32[4,544,544]{1,2,0:T(8,128)S(1)}) fusion(f32[4,544,544]{1,2,0:T(8,128)} %get-tuple-element.61, f32[4,544]{1,0:T(4,128)S(1)} %get-tuple-element.60, bf16[544,4,64]{0,2,1:T(8,128)(2,1)S(1)} %copy.67, bf16[544,4,64]{2,1,0:T(4,128)(2,1)S(1)} %reshape.151), kind=kOutput, calls=%fused_computation.2 | convolution fusion | flops 155068288 | bytes 10044416 | tf_op jit(solution)/shard_map/qhd,khd->hqk/dot_general | solution.py:37
  80.2 3.6 %multiply_convert_fusion = bf16[4,544,544]{1,2,0:T(8,128)(2,1)S(1)} fusion(f32[4,544,544]{1,2,0:T(8,128)S(1)} %get-tuple-element.63, f32[4,544]{1,0:T(4,128)S(1)} %get-tuple-element.62, f32[4,544,544]{1,2,0:T(8,128)} %get-tuple-element.61, f32[4,544]{1,0:T(4,128)S(1)} %get-tuple-element.60), kind=kLoop, calls=%fused_computation.1 | loop fusion | flops 4734976 | bytes 11854848 | tf_op jit(solution)/shard_map/convert_element_type | solution.py:41
  83.8 1.7 fusion.15
  85.5 1.3 reshape.153
  87.8 12.1 %all-to-all-done.7 = bf16[136,4,512]{2,0,1:T(8,128)(2,1)} async-done(((bf16[136,4,512]{2,0,1:T(8,128)(2,1)}), bf16[136,4,512]{2,0,1:T(8,128)(2,1)}, u32[]{:S(2)}, u32[]{:S(2)}) %all-to-all-start.7) | async-done | bytes 557088 | tf_op jit(solution)/shard_map/all_to_all | solution.py:62
  99.9 4.1 %all-to-all-start.5 = ((bf16[4,136,256]{2,1,0:T(8,128)(2,1)}), bf16[4,136,256]{2,1,0:T(8,128)(2,1)}, u32[]{:S(2)}, u32[]{:S(2)}) async-start(bf16[4,136,256]{2,1,0:T(8,128)(2,1)} %copy.86), calls=%async_computation.5 | async-start | bytes 557056 | tf_op jit(solution)/shard_map/all_to_all | solution.py:90
  104.3 3.4 %convolution_convert_fusion = bf16[1024,512]{1,0:T(8,128)(2,1)} fusion(bf16[544,1024]{0,1:T(8,128)(2,1)} %all-gather.3.cloned.1.call-done, bf16[544,512]{1,0:T(8,128)(2,1)} %bitcast.14), kind=kOutput, calls=%fused_computation.14 | convolution fusion | flops 570949632 | bytes 2719744 | tf_op jit(solution)/shard_map/dot_general | solution.py:80
  111.0 3.6 %all-to-all-start.4 = ((bf16[4,136,256]{2,1,0:T(8,128)(2,1)}), bf16[4,136,256]{2,1,0:T(8,128)(2,1)S(1)}, u32[]{:S(2)}, u32[]{:S(2)}) async-start(bf16[4,136,256]{2,1,0:T(8,128)(2,1)} %copy.85), calls=%async_computation.4 | async-start | bytes 557056 | tf_op jit(solution)/shard_map/all_to_all | solution.py:89
  114.6 9.8 %all-gather.5.cloned.1.call-done = bf16[512,1024]{1,0:T(8,128)(2,1)} async-done(((bf16[512,128]{1,0:T(8,128)(2,1)}), bf16[512,1024]{1,0:T(8,128)(2,1)}) %all-gather.5.cloned.1.call-update) | async-done | bytes 1048592 | tf_op jit(solution)/shard_map/all_gather | solution.py:78
  124.4 3.4 %convolution_convert_fusion.1 = bf16[544,512]{1,0:T(8,128)(2,1)} fusion(bf16[544,1024]{0,1:T(8,128)(2,1)} %all-gather.3.cloned.1.call-done, bf16[512,1024]{1,0:T(8,128)(2,1)} %all-gather.5.cloned.1.call-done), kind=kOutput, calls=%fused_computation.16 | convolution fusion | flops 570703872 | bytes 2719744 | tf_op jit(solution)/shard_map/dot_general | solution.py:92
  127.8 4.6 %all-to-all-start.6 = ((bf16[4,136,512]{2,1,0:T(8,128)(2,1)}), bf16[4,136,512]{2,1,0:T(8,128)(2,1)S(1)}, u32[]{:S(2)}, u32[]{:S(2)}) async-start(bf16[4,136,512]{2,1,0:T(8,128)(2,1)} %bitcast.11), calls=%async_computation.6 | async-start | bytes 1114112 | tf_op jit(solution)/shard_map/all_to_all | solution.py:95
  135.4 12.6 %all-to-all-done.6 = bf16[4,136,512]{2,1,0:T(8,128)(2,1)S(1)} async-done(((bf16[4,136,512]{2,1,0:T(8,128)(2,1)}), bf16[4,136,512]{2,1,0:T(8,128)(2,1)S(1)}, u32[]{:S(2)}, u32[]{:S(2)}) %all-to-all-start.6) | async-done | bytes 557088 | tf_op jit(solution)/shard_map/all_to_all | solution.py:95
  149.5 14.1 %reduce-scatter.2.cloned.1.call-done = bf16[128,512]{1,0:T(8,128)(2,1)} async-done(((bf16[1024,512]{1,0:T(8,128)(2,1)}), bf16[128,512]{1,0:T(8,128)(2,1)}) %reduce-scatter.2.cloned.1.call-update) | async-done | bytes 131088 | tf_op jit(solution)/shard_map/reduce_scatter | solution.py:79
  (49 shorter events, 21.7 us)
Async XLA Ops:
  7.2 39.1 %copy-start.4 = (f32[1,4,544]{2,1,0:T(4,128)S(1)}, f32[1,4,544]{2,1,0:T(4,128)}, u32[]{:S(2)}) copy-start(f32[1,4,544]{2,1,0:T(4,128)} %param.20) | copy-start | bytes 26116
  9.1 15.6 %all-to-all-start = ((bf16[136,4,256]{2,0,1:T(8,128)(2,1)}), bf16[136,4,256]{2,0,1:T(8,128)(2,1)S(1)}, u32[]{:S(2)}, u32[]{:S(2)}) async-start(bf16[136,4,256]{2,0,1:T(8,128)(2,1)} %copy.61), calls=%async_computation | async-start | bytes 557056 | tf_op jit(solution)/shard_map/all_to_all | solution.py:58
  24.7 10.6 %all-to-all-start.1 = ((bf16[136,4,256]{2,0,1:T(8,128)(2,1)}), bf16[136,4,256]{2,0,1:T(8,128)(2,1)S(1)}, u32[]{:S(2)}, u32[]{:S(2)}) async-start(bf16[136,4,256]{2,0,1:T(8,128)(2,1)} %copy.62), calls=%async_computation.1 | async-start | bytes 557056 | tf_op jit(solution)/shard_map/all_to_all | solution.py:59
  35.3 10.3 %all-to-all-start.2 = ((bf16[136,4,256]{2,0,1:T(8,128)(2,1)}), bf16[136,4,256]{2,0,1:T(8,128)(2,1)S(1)}, u32[]{:S(2)}, u32[]{:S(2)}) async-start(bf16[136,4,256]{2,0,1:T(8,128)(2,1)} %copy.65), calls=%async_computation.2 | async-start | bytes 557056 | tf_op jit(solution)/shard_map/all_to_all | solution.py:61
  38.7 65.5 %all-gather.3.cloned.1.call-start = ((), (), s32[]{:S(2)}) async-start(), calls=%async_computation.9 | async-start | bytes 1638400 | tf_op jit(solution)/shard_map/all_gather | solution.py:77
  40.2 10.5 %copy-start = (bf16[544,4,64]{0,2,1:T(8,128)(2,1)}, bf16[544,4,64]{0,2,1:T(8,128)(2,1)S(1)}, u32[]{:S(2)}) copy-start(bf16[544,4,64]{0,2,1:T(8,128)(2,1)S(1)} %copy.64) | copy-start | bytes 835588
  50.6 3.9 %copy-start.3 = (bf16[1,136,1024]{2,1,0:T(8,128)(2,1)S(1)}, bf16[1,136,1024]{2,1,0:T(8,128)(2,1)}, u32[]{:S(2)}) copy-start(bf16[1,136,1024]{2,1,0:T(8,128)(2,1)} %param.18) | copy-start | bytes 835588
  50.6 9.0 %copy-start.2 = (bf16[1,136,2048]{2,1,0:T(8,128)(2,1)S(1)}, bf16[1,136,2048]{2,1,0:T(8,128)(2,1)}, u32[]{:S(2)}) copy-start(bf16[1,136,2048]{2,1,0:T(8,128)(2,1)} %param.15) | copy-start | bytes 1671172
  55.4 10.5 %all-to-all-start.3 = ((bf16[136,4,256]{2,0,1:T(8,128)(2,1)}), bf16[136,4,256]{2,0,1:T(8,128)(2,1)S(1)}, u32[]{:S(2)}, u32[]{:S(2)}) async-start(bf16[136,4,256]{2,0,1:T(8,128)(2,1)} %copy.66), calls=%async_computation.3 | async-start | bytes 557056 | tf_op jit(solution)/shard_map/all_to_all | solution.py:60
  58.9 65.5 %all-gather.5.cloned.1.call-start = ((), (), s32[]{:S(2)}) async-start(), calls=%async_computation.10 | async-start | bytes 1179648 | tf_op jit(solution)/shard_map/all_gather | solution.py:78
  65.9 34.0 %all-to-all-start.7 = ((bf16[136,4,512]{2,0,1:T(8,128)(2,1)}), bf16[136,4,512]{2,0,1:T(8,128)(2,1)}, u32[]{:S(2)}, u32[]{:S(2)}) async-start(bf16[136,4,512]{2,0,1:T(8,128)(2,1)} %copy.80), calls=%async_computation.7 | async-start | bytes 1114112 | tf_op jit(solution)/shard_map/all_to_all | solution.py:62
  87.8 19.9 %copy-start.1 = (bf16[544,4,64]{0,2,1:T(8,128)(2,1)S(1)}, bf16[544,4,64]{0,2,1:T(8,128)(2,1)}, u32[]{:S(2)}) copy-start(bf16[544,4,64]{0,2,1:T(8,128)(2,1)} %copy-done) | copy-start | bytes 835588
  99.9 11.1 %all-to-all-start.5 = ((bf16[4,136,256]{2,1,0:T(8,128)(2,1)}), bf16[4,136,256]{2,1,0:T(8,128)(2,1)}, u32[]{:S(2)}, u32[]{:S(2)}) async-start(bf16[4,136,256]{2,1,0:T(8,128)(2,1)} %copy.86), calls=%async_computation.5 | async-start | bytes 557056 | tf_op jit(solution)/shard_map/all_to_all | solution.py:90
  104.0 59.6 %reduce-scatter.2.cloned.1.call-start = ((), (), s32[]{:S(2)}) async-start(), calls=%async_computation.11 | async-start | bytes 1179648 | tf_op jit(solution)/shard_map/reduce_scatter | solution.py:79
  111.0 16.8 %all-to-all-start.4 = ((bf16[4,136,256]{2,1,0:T(8,128)(2,1)}), bf16[4,136,256]{2,1,0:T(8,128)(2,1)S(1)}, u32[]{:S(2)}, u32[]{:S(2)}) async-start(bf16[4,136,256]{2,1,0:T(8,128)(2,1)} %copy.85), calls=%async_computation.4 | async-start | bytes 557056 | tf_op jit(solution)/shard_map/all_to_all | solution.py:89
  127.8 20.2 %all-to-all-start.6 = ((bf16[4,136,512]{2,1,0:T(8,128)(2,1)}), bf16[4,136,512]{2,1,0:T(8,128)(2,1)S(1)}, u32[]{:S(2)}, u32[]{:S(2)}) async-start(bf16[4,136,512]{2,1,0:T(8,128)(2,1)} %bitcast.11), calls=%async_computation.6 | async-start | bytes 1114112 | tf_op jit(solution)/shard_map/all_to_all | solution.py:95
Sparse Core Ops, SparseCore 0:
  54.6 45.5 all-gather.2
  102.0 22.3 all-gather.4
  127.6 35.9 reduce-scatter.1
where the time goes:
time: 173 us; the launch traced here: 172 us
  waiting for transfers between devices  73.5 us (42%)
  starting transfers between devices  39.8 us (23%)
  matrix products  20.9 us (12%)
  local copies, waits for them, and re-layouts  19.1 us (11%)
  between operations  14 us (8%)
  other arithmetic  4.58 us (3%)
    reduce_scatter x1, waiting for transfers between devices, shards(): lax.psum_scatter(lax.dot_general(value_all, input_cols, (((0,), (0,)), ((...  14.1 us
    all_to_all x1, waiting for transfers between devices, shards(): lax.all_to_all(column_grad, 'sp', split_axis=0, concat_axis=1, tiled=True)  12.6 us
    all_to_all x1, waiting for transfers between devices, shards(): lax.all_to_all(inputs[0], 'sp', split_axis=1, concat_axis=0, tiled=True)  12.1 us
    all_to_all x1, starting transfers between devices, shards(): lax.all_to_all(inputs[0], 'sp', split_axis=1, concat_axis=0, tiled=True)  10.5 us
    all_gather x1, waiting for transfers between devices, shards(): weight_block = lax.all_gather(value_weight, 'dp', axis=1, tiled=True)  9.81 us
    all_to_all x1, waiting for transfers between devices, shards(): lax.all_to_all(query_vectors[0], 'sp', split_axis=1, concat_axis=0, tiled...  7.36 us
    all_to_all x1, starting transfers between devices, shards(): lax.all_to_all(query_vectors[0], 'sp', split_axis=1, concat_axis=0, tiled...  6.35 us
    all_to_all x1, waiting for transfers between devices, shards(): lax.all_to_all(cotangent[0], 'sp', split_axis=1, concat_axis=0, tiled=True)  5.43 us
  transfers between devices with their start and end apart: 11, of which 9 were waited for; matrix products, arithmetic and copies ran while one was open for 17% of the time, Pallas kernels for 0%

commit v1 on v0

--- a/solution.py
+++ b/solution.py
@@ -75,7 +75,12 @@
     key_flat = key_heads.reshape(length, local_width)
     value_flat = value_heads.reshape(length, local_width)
     value_all = lax.all_gather(value_flat, "sp", axis=1, tiled=True)
-    weight_block = lax.all_gather(value_weight, "dp", axis=1, tiled=True)
+    ring = [value_weight]
+    for hop in range(7):
+        ring.append(lax.ppermute(ring[-1], "dp", [(dev, (dev + 1) % 8) for dev in range(8)]))
+    weight_block = jnp.roll(
+        jnp.concatenate(ring[::-1], axis=1), (lax.axis_index("dp") + 1) * ring[0].shape[1], axis=1
+    )
     weight_rows = lax.psum_scatter(
         lax.dot_general(
             value_all, input_cols, (((0,), (0,)), ((), ())), preferred_element_type=jnp.float32

time: 173 us -> 164 us (0.948)
  local copies, waits for them, and re-layouts: 19.1 us -> 28.4 us
  waiting for transfers between devices: 73.5 us -> 64.4 us
  starting transfers between devices: 39.8 us -> 33.9 us
  other arithmetic: 4.58 us -> 1.92 us
    ppermute x0 -> x7, waiting for transfers between devices: none -> 24.4 us  [shards(): lax.ppermute(ring[-1], 'dp', [(dev, (dev + 1) % 8) for dev in range(8)])]
    all_to_all x1, waiting for transfers between devices: 12.1 us -> 0.01 us  [shards(): lax.all_to_all(inputs[0], 'sp', split_axis=1, concat_axis=0, tiled=True)]
    reduce_scatter x1, waiting for transfers between devices: 14.1 us -> 3.18 us  [shards(): lax.psum_scatter(lax.dot_general(value_all, input_cols, (((0,), (0,)), ((...]
    unnamed x11 -> x34, local copies, waits for them, and re-layouts: 0.86 us -> 11.6 us
    all_gather x1 -> x0, waiting for transfers between devices: 9.81 us -> none  [shards(): weight_block = lax.all_gather(value_weight, 'dp', axis=1, tiled=True)]
    all_to_all x1, starting transfers between devices: 10.5 us -> 5.05 us  [shards(): lax.all_to_all(inputs[0], 'sp', split_axis=1, concat_axis=0, tiled=True)]
    all_to_all x1, waiting for transfers between devices: 4.95 us -> 0.01 us  [shards(): lax.all_to_all(value_vectors[0], 'sp', split_axis=1, concat_axis=0, tiled...]
    all_to_all x1, starting transfers between devices: 6.35 us -> 3.45 us  [shards(): lax.all_to_all(query_vectors[0], 'sp', split_axis=1, concat_axis=0, tiled...]
  transfers between devices with their start and end apart: 11 -> 17, of which waited for: 9 -> 13; matrix products, arithmetic and copies ran while one was open for 17% -> 27% of each run, Pallas kernels for 0% -> 0%
where the time goes in v1:
time: 164 us; the launch traced here: 163 us
  waiting for transfers between devices  64.4 us (39%)
  starting transfers between devices  33.9 us (21%)
  local copies, waits for them, and re-layouts  28.4 us (17%)
  matrix products  19.7 us (12%)
  between operations  14.3 us (9%)
  other arithmetic  1.92 us (1%)
    ppermute x7, waiting for transfers between devices, shards(): lax.ppermute(ring[-1], 'dp', [(dev, (dev + 1) % 8) for dev in range(8)])  24.4 us
    unnamed x34, local copies, waits for them, and re-layouts  11.6 us
    all_to_all x1, waiting for transfers between devices, shards(): lax.all_to_all(column_grad, 'sp', split_axis=0, concat_axis=1, tiled=True)  11 us
    all_to_all x1, waiting for transfers between devices, shards(): lax.all_to_all(key_vectors[0], 'sp', split_axis=1, concat_axis=0, tiled=T...  7.35 us
    all_to_all x1, starting transfers between devices, shards(): lax.all_to_all(key_vectors[0], 'sp', split_axis=1, concat_axis=0, tiled=T...  6.35 us
    all_to_all x1, waiting for transfers between devices, shards(): lax.all_to_all(query_vectors[0], 'sp', split_axis=1, concat_axis=0, tiled...  6.18 us
    all_to_all x1, waiting for transfers between devices, shards(): lax.all_to_all(cotangent[0], 'sp', split_axis=1, concat_axis=0, tiled=True)  5.93 us
    all_to_all x1, starting transfers between devices, shards(): lax.all_to_all(query_flat, 'sp', split_axis=0, concat_axis=1, tiled=True)  5.09 us
  transfers between devices with their start and end apart: 17, of which 13 were waited for; matrix products, arithmetic and copies ran while one was open for 27% of the time, Pallas kernels for 0%

profile of v1, /device:TPU:0, one launch (start us, length us, event | category | flops | bytes accessed | tf_op | source)
XLA Modules:
  0.0 162.7 jit_solution(5597326827481229056)
XLA Ops:
  9.1 6.3 %all-to-all-start.1 = ((bf16[136,4,256]{2,0,1:T(8,128)(2,1)}), bf16[136,4,256]{2,0,1:T(8,128)(2,1)S(1)}, u32[]{:S(2)}, u32[]{:S(2)}) async-start(bf16[136,4,256]{2,0,1:T(8,128)(2,1)} %copy.62), calls=%async_computation.1 | async-start | bytes 557056 | tf_op jit(solution)/shard_map/all_to_all | solution.py:59
  17.4 7.3 %all-to-all-done.1 = bf16[136,4,256]{2,0,1:T(8,128)(2,1)S(1)} async-done(((bf16[136,4,256]{2,0,1:T(8,128)(2,1)}), bf16[136,4,256]{2,0,1:T(8,128)(2,1)S(1)}, u32[]{:S(2)}, u32[]{:S(2)}) %all-to-all-start.1) | async-done | bytes 278560 | tf_op jit(solution)/shard_map/all_to_all | solution.py:59
  24.7 3.5 %all-to-all-start = ((bf16[136,4,256]{2,0,1:T(8,128)(2,1)}), bf16[136,4,256]{2,0,1:T(8,128)(2,1)S(1)}, u32[]{:S(2)}, u32[]{:S(2)}) async-start(bf16[136,4,256]{2,0,1:T(8,128)(2,1)} %copy.61), calls=%async_computation | async-start | bytes 557056 | tf_op jit(solution)/shard_map/all_to_all | solution.py:58
  29.1 6.2 %all-to-all-done = bf16[136,4,256]{2,0,1:T(8,128)(2,1)S(1)} async-done(((bf16[136,4,256]{2,0,1:T(8,128)(2,1)}), bf16[136,4,256]{2,0,1:T(8,128)(2,1)S(1)}, u32[]{:S(2)}, u32[]{:S(2)}) %all-to-all-start) | async-done | bytes 278560 | tf_op jit(solution)/shard_map/all_to_all | solution.py:58
  35.3 3.5 %all-to-all-start.2 = ((bf16[136,4,256]{2,0,1:T(8,128)(2,1)}), bf16[136,4,256]{2,0,1:T(8,128)(2,1)S(1)}, u32[]{:S(2)}, u32[]{:S(2)}) async-start(bf16[136,4,256]{2,0,1:T(8,128)(2,1)} %copy.65), calls=%async_computation.2 | async-start | bytes 557056 | tf_op jit(solution)/shard_map/all_to_all | solution.py:61
  39.7 5.9 %all-to-all-done.2 = bf16[136,4,256]{2,0,1:T(8,128)(2,1)S(1)} async-done(((bf16[136,4,256]{2,0,1:T(8,128)(2,1)}), bf16[136,4,256]{2,0,1:T(8,128)(2,1)S(1)}, u32[]{:S(2)}, u32[]{:S(2)}) %all-to-all-start.2) | async-done | bytes 278560 | tf_op jit(solution)/shard_map/all_to_all | solution.py:61
  45.7 3.5 %all-to-all-start.3 = ((bf16[136,4,256]{2,0,1:T(8,128)(2,1)}), bf16[136,4,256]{2,0,1:T(8,128)(2,1)S(1)}, u32[]{:S(2)}, u32[]{:S(2)}) async-start(bf16[136,4,256]{2,0,1:T(8,128)(2,1)} %copy.66), calls=%async_computation.3 | async-start | bytes 557056 | tf_op jit(solution)/shard_map/all_to_all | solution.py:60
  49.2 5.3 %collective-permute-done = bf16[512,128]{1,0:T(8,128)(2,1)S(1)} collective-permute-done((bf16[512,128]{1,0:T(8,128)(2,1)S(1)}, bf16[512,128]{1,0:T(8,128)(2,1)S(1)}, u32[]{:S(2)}, u32[]{:S(2)}) %collective-permute-start) | collective-permute-done | bytes 131104 | tf_op jit(solution)/shard_map/ppermute | solution.py:80
  54.5 5.3 %collective-permute-done.1 = bf16[512,128]{1,0:T(8,128)(2,1)S(1)} collective-permute-done((bf16[512,128]{1,0:T(8,128)(2,1)S(1)}, bf16[512,128]{1,0:T(8,128)(2,1)S(1)}, u32[]{:S(2)}, u32[]{:S(2)}) %collective-permute-start.1) | collective-permute-done | bytes 131104 | tf_op jit(solution)/shard_map/ppermute | solution.py:80
  61.2 3.9 %collective-permute-done.2 = bf16[512,128]{1,0:T(8,128)(2,1)S(1)} collective-permute-done((bf16[512,128]{1,0:T(8,128)(2,1)S(1)}, bf16[512,128]{1,0:T(8,128)(2,1)S(1)}, u32[]{:S(2)}, u32[]{:S(2)}) %collective-permute-start.2) | collective-permute-done | bytes 131104 | tf_op jit(solution)/shard_map/ppermute | solution.py:80
  67.7 5.0 %all-to-all-start.7 = ((bf16[136,4,512]{2,0,1:T(8,128)(2,1)}), bf16[136,4,512]{2,0,1:T(8,128)(2,1)S(1)}, u32[]{:S(2)}, u32[]{:S(2)}) async-start(bf16[136,4,512]{2,0,1:T(8,128)(2,1)} %copy.80), calls=%async_computation.7 | async-start | bytes 1114112 | tf_op jit(solution)/shard_map/all_to_all | solution.py:62
  73.0 4.3 %fusion.24 = (f32[4,544]{1,0:T(4,128)S(1)}, f32[4,544,544]{1,2,0:T(8,128)}) fusion(f32[4,544]{1,0:T(4,128)S(1)} %bitcast.49, pred[544,544]{0,1:T(8,128)(4,1)S(1)} %iota_compare_fusion, bf16[544,4,64]{0,2,1:T(8,128)(2,1)S(1)} %copy.63, bf16[544,4,64]{0,2,1:T(8,128)(2,1)S(1)} %copy.64), kind=kOutput, calls=%fused_computation.48 | convolution fusion | flops 158622240 | bytes 5605376 | tf_op jit(solution)/shard_map/sub | solution.py:31
  77.3 3.8 %fusion.11 = bf16[4,544,64]{1,2,0:T(8,128)(2,1)} fusion(bf16[544,4,64]{0,2,1:T(8,128)(2,1)S(1)} %copy-done.2, f32[4,544]{1,0:T(4,128)S(1)} %get-tuple-element.60, f32[4,544]{1,0:T(4,128)S(1)} %bitcast.50, pred[544,544]{0,1:T(8,128)(4,1)S(1)} %iota_compare_fusion, bf16[544,4,64]{0,2,1:T(8,128)(2,1)S(1)} %copy.63, bf16[544,4,64]{0,2,1:T(8,128)(2,1)S(1)} %copy.64), kind=kOutput, calls=%fused_computation.21 | convolution fusion | flops 311466656 | bytes 1427456 | tf_op jit(solution)/shard_map/hqk,qhd->khd/dot_general | solution.py:35
  81.2 3.6 %multiply_reduce_fusion = (f32[4,544]{1,0:T(4,128)S(1)}, f32[4,544,544]{1,2,0:T(8,128)S(1)}) fusion(f32[4,544,544]{1,2,0:T(8,128)} %get-tuple-element.61, f32[4,544]{1,0:T(4,128)S(1)} %get-tuple-element.60, bf16[544,4,64]{0,2,1:T(8,128)(2,1)S(1)} %copy-done.2, bf16[544,4,64]{2,1,0:T(4,128)(2,1)S(1)} %reshape.151), kind=kOutput, calls=%fused_computation.2 | convolution fusion | flops 155068288 | bytes 10044416 | tf_op jit(solution)/shard_map/qhd,khd->hqk/dot_general | solution.py:37
  86.3 3.9 %collective-permute-done.4 = bf16[512,128]{1,0:T(8,128)(2,1)S(1)} collective-permute-done((bf16[512,128]{1,0:T(8,128)(2,1)S(1)}, bf16[512,128]{1,0:T(8,128)(2,1)S(1)}, u32[]{:S(2)}, u32[]{:S(2)}) %collective-permute-start.4) | collective-permute-done | bytes 131104 | tf_op jit(solution)/shard_map/ppermute | solution.py:80
  90.8 4.6 %collective-permute-done.5 = bf16[512,128]{1,0:T(8,128)(2,1)S(1)} collective-permute-done((bf16[512,128]{1,0:T(8,128)(2,1)S(1)}, bf16[512,128]{1,0:T(8,128)(2,1)S(1)}, u32[]{:S(2)}, u32[]{:S(2)}) %collective-permute-start.5) | collective-permute-done | bytes 131104 | tf_op jit(solution)/shard_map/ppermute | solution.py:80
  108.3 5.1 %all-to-all-start.4 = ((bf16[4,136,256]{2,1,0:T(8,128)(2,1)}), bf16[4,136,256]{2,1,0:T(8,128)(2,1)S(1)}, u32[]{:S(2)}, u32[]{:S(2)}) async-start(bf16[4,136,256]{2,1,0:T(8,128)(2,1)} %copy.85), calls=%async_computation.4 | async-start | bytes 557056 | tf_op jit(solution)/shard_map/all_to_all | solution.py:94
  116.2 3.3 %convolution_convert_fusion = bf16[1024,512]{1,0:T(8,128)(2,1)} fusion(bf16[544,1024]{0,1:T(8,128)(2,1)} %all-gather.2.cloned.1.call-done, bf16[544,512]{1,0:T(8,128)(2,1)S(1)} %bitcast.47), kind=kOutput, calls=%fused_computation.14 | convolution fusion | flops 570949632 | bytes 2719744 | tf_op jit(solution)/shard_map/dot_general | solution.py:85
  121.5 3.5 %all-to-all-start.5 = ((bf16[4,136,256]{2,1,0:T(8,128)(2,1)}), bf16[4,136,256]{2,1,0:T(8,128)(2,1)S(1)}, u32[]{:S(2)}, u32[]{:S(2)}) async-start(bf16[4,136,256]{2,1,0:T(8,128)(2,1)} %copy.86), calls=%async_computation.5 | async-start | bytes 557056 | tf_op jit(solution)/shard_map/all_to_all | solution.py:95
  126.4 3.0 %convolution_convert_fusion.1 = bf16[544,512]{1,0:T(8,128)(2,1)} fusion(bf16[544,1024]{0,1:T(8,128)(2,1)S(1)} %copy-done.5, bf16[512,2048]{1,0:T(8,128)(2,1)} %constant_dynamic-update-slice_fusion, s32[]{:T(128)S(6)} %select_n.19), kind=kOutput, calls=%fused_computation.16 | convolution fusion | flops 570703872 | bytes 2719748 | tf_op jit(solution)/shard_map/dot_general | solution.py:97
  129.4 3.6 %all-to-all-done.5 = bf16[4,136,256]{2,1,0:T(8,128)(2,1)S(1)} async-done(((bf16[4,136,256]{2,1,0:T(8,128)(2,1)}), bf16[4,136,256]{2,1,0:T(8,128)(2,1)S(1)}, u32[]{:S(2)}, u32[]{:S(2)}) %all-to-all-start.5) | async-done | bytes 278560 | tf_op jit(solution)/shard_map/all_to_all | solution.py:95
  133.0 3.5 %all-to-all-start.6 = ((bf16[4,136,512]{2,1,0:T(8,128)(2,1)}), bf16[4,136,512]{2,1,0:T(8,128)(2,1)S(1)}, u32[]{:S(2)}, u32[]{:S(2)}) async-start(bf16[4,136,512]{2,1,0:T(8,128)(2,1)} %bitcast.11), calls=%async_computation.6 | async-start | bytes 1114112 | tf_op jit(solution)/shard_map/all_to_all | solution.py:100
  138.5 11.0 %all-to-all-done.6 = bf16[4,136,512]{2,1,0:T(8,128)(2,1)S(1)} async-done(((bf16[4,136,512]{2,1,0:T(8,128)(2,1)}), bf16[4,136,512]{2,1,0:T(8,128)(2,1)S(1)}, u32[]{:S(2)}, u32[]{:S(2)}) %all-to-all-start.6) | async-done | bytes 557088 | tf_op jit(solution)/shard_map/all_to_all | solution.py:100
  150.9 3.2 %reduce-scatter.2.cloned.1.call-done = bf16[128,512]{1,0:T(8,128)(2,1)} async-done(((bf16[1024,512]{1,0:T(8,128)(2,1)}), bf16[128,512]{1,0:T(8,128)(2,1)}) %reduce-scatter.2.cloned.1.call-update) | async-done | bytes 131088 | tf_op jit(solution)/shard_map/reduce_scatter | solution.py:84
  (85 shorter events, 36.5 us)
Async XLA Ops:
  7.2 21.0 %copy-start.3 = (bf16[1,136,1024]{2,1,0:T(8,128)(2,1)S(1)}, bf16[1,136,1024]{2,1,0:T(8,128)(2,1)}, u32[]{:S(2)}) copy-start(bf16[1,136,1024]{2,1,0:T(8,128)(2,1)} %param.19) | copy-start | bytes 835588
  8.4 30.4 %copy-start.4 = (bf16[1,136,1024]{2,1,0:T(8,128)(2,1)S(1)}, bf16[1,136,1024]{2,1,0:T(8,128)(2,1)}, u32[]{:S(2)}) copy-start(bf16[1,136,1024]{2,1,0:T(8,128)(2,1)} %param.18) | copy-start | bytes 835588
  9.1 15.6 %all-to-all-start.1 = ((bf16[136,4,256]{2,0,1:T(8,128)(2,1)}), bf16[136,4,256]{2,0,1:T(8,128)(2,1)S(1)}, u32[]{:S(2)}, u32[]{:S(2)}) async-start(bf16[136,4,256]{2,0,1:T(8,128)(2,1)} %copy.62), calls=%async_computation.1 | async-start | bytes 557056 | tf_op jit(solution)/shard_map/all_to_all | solution.py:59
  16.6 32.5 %copy-start.1 = (bf16[512,128]{1,0:T(8,128)(2,1)S(1)}, bf16[512,128]{1,0:T(8,128)(2,1)}, u32[]{:S(2)}) copy-start(bf16[512,128]{1,0:T(8,128)(2,1)} %param.21) | copy-start | bytes 393220
  17.4 42.4 %copy-start = (bf16[1,136,2048]{2,1,0:T(8,128)(2,1)S(1)}, bf16[1,136,2048]{2,1,0:T(8,128)(2,1)}, u32[]{:S(2)}) copy-start(bf16[1,136,2048]{2,1,0:T(8,128)(2,1)} %param.15) | copy-start | bytes 1671172
  24.7 10.6 %all-to-all-start = ((bf16[136,4,256]{2,0,1:T(8,128)(2,1)}), bf16[136,4,256]{2,0,1:T(8,128)(2,1)S(1)}, u32[]{:S(2)}, u32[]{:S(2)}) async-start(bf16[136,4,256]{2,0,1:T(8,128)(2,1)} %copy.61), calls=%async_computation | async-start | bytes 557056 | tf_op jit(solution)/shard_map/all_to_all | solution.py:58
  35.3 10.3 %all-to-all-start.2 = ((bf16[136,4,256]{2,0,1:T(8,128)(2,1)}), bf16[136,4,256]{2,0,1:T(8,128)(2,1)S(1)}, u32[]{:S(2)}, u32[]{:S(2)}) async-start(bf16[136,4,256]{2,0,1:T(8,128)(2,1)} %copy.65), calls=%async_computation.2 | async-start | bytes 557056 | tf_op jit(solution)/shard_map/all_to_all | solution.py:61
  45.7 22.0 %all-to-all-start.3 = ((bf16[136,4,256]{2,0,1:T(8,128)(2,1)}), bf16[136,4,256]{2,0,1:T(8,128)(2,1)S(1)}, u32[]{:S(2)}, u32[]{:S(2)}) async-start(bf16[136,4,256]{2,0,1:T(8,128)(2,1)} %copy.66), calls=%async_computation.3 | async-start | bytes 557056 | tf_op jit(solution)/shard_map/all_to_all | solution.py:60
  49.1 5.3 %collective-permute-start = (bf16[512,128]{1,0:T(8,128)(2,1)S(1)}, bf16[512,128]{1,0:T(8,128)(2,1)S(1)}, u32[]{:S(2)}, u32[]{:S(2)}) collective-permute-start(bf16[512,128]{1,0:T(8,128)(2,1)S(1)} %copy-done.1), channel_id=1, source_target_pairs={{0,1},{1,2},{2,3},{3,4},{4,5},{5,6},{6,7},{7,0},{8,9},{9,10},{10,1... | collective-permute-start | bytes 393224 | tf_op jit(solution)/shard_map/ppermute | solution.py:80
  54.5 5.3 %collective-permute-start.1 = (bf16[512,128]{1,0:T(8,128)(2,1)S(1)}, bf16[512,128]{1,0:T(8,128)(2,1)S(1)}, u32[]{:S(2)}, u32[]{:S(2)}) collective-permute-start(bf16[512,128]{1,0:T(8,128)(2,1)S(1)} %collective-permute-done), channel_id=1, source_target_pairs={{0,1},{1,2},{2,3},{3,4},{4,5},{5,6},{6,7},{7,0},{8,9},{9,10},{10,1... | collective-permute-start | bytes 393224 | tf_op jit(solution)/shard_map/ppermute | solution.py:80
  59.8 5.3 %collective-permute-start.2 = (bf16[512,128]{1,0:T(8,128)(2,1)S(1)}, bf16[512,128]{1,0:T(8,128)(2,1)S(1)}, u32[]{:S(2)}, u32[]{:S(2)}) collective-permute-start(bf16[512,128]{1,0:T(8,128)(2,1)S(1)} %collective-permute-done.1), channel_id=1, source_target_pairs={{0,1},{1,2},{2,3},{3,4},{4,5},{5,6},{6,7},{7,0},{8,9},{9,10},{10,1... | collective-permute-start | bytes 393224 | tf_op jit(solution)/shard_map/ppermute | solution.py:80
  65.1 19.8 %collective-permute-start.3 = (bf16[512,128]{1,0:T(8,128)(2,1)S(1)}, bf16[512,128]{1,0:T(8,128)(2,1)S(1)}, u32[]{:S(2)}, u32[]{:S(2)}) collective-permute-start(bf16[512,128]{1,0:T(8,128)(2,1)S(1)} %collective-permute-done.2), channel_id=1, source_target_pairs={{0,1},{1,2},{2,3},{3,4},{4,5},{5,6},{6,7},{7,0},{8,9},{9,10},{10,1... | collective-permute-start | bytes 393224 | tf_op jit(solution)/shard_map/ppermute | solution.py:80
  66.0 7.0 %copy-start.6 = (f32[1,4,544]{2,1,0:T(4,128)S(1)}, f32[1,4,544]{2,1,0:T(4,128)}, u32[]{:S(2)}) copy-start(f32[1,4,544]{2,1,0:T(4,128)} %param.20) | copy-start | bytes 26116
  67.7 40.6 %all-to-all-start.7 = ((bf16[136,4,512]{2,0,1:T(8,128)(2,1)}), bf16[136,4,512]{2,0,1:T(8,128)(2,1)S(1)}, u32[]{:S(2)}, u32[]{:S(2)}) async-start(bf16[136,4,512]{2,0,1:T(8,128)(2,1)} %copy.80), calls=%async_computation.7 | async-start | bytes 1114112 | tf_op jit(solution)/shard_map/all_to_all | solution.py:62
  72.7 43.4 %all-gather.2.cloned.1.call-start = ((), (), s32[]{:S(2)}) async-start(), calls=%async_computation.9 | async-start | bytes 1638400 | tf_op jit(solution)/shard_map/all_gather | solution.py:77
  73.0 4.3 %copy-start.2 = (bf16[544,4,64]{0,2,1:T(8,128)(2,1)S(1)}, bf16[544,4,64]{0,2,1:T(8,128)(2,1)}, u32[]{:S(2)}) copy-start(bf16[544,4,64]{0,2,1:T(8,128)(2,1)} %copy.67) | copy-start | bytes 835588
  84.8 5.3 %collective-permute-start.4 = (bf16[512,128]{1,0:T(8,128)(2,1)S(1)}, bf16[512,128]{1,0:T(8,128)(2,1)S(1)}, u32[]{:S(2)}, u32[]{:S(2)}) collective-permute-start(bf16[512,128]{1,0:T(8,128)(2,1)S(1)} %collective-permute-done.3), channel_id=1, source_target_pairs={{0,1},{1,2},{2,3},{3,4},{4,5},{5,6},{6,7},{7,0},{8,9},{9,10},{10,1... | collective-permute-start | bytes 393224 | tf_op jit(solution)/shard_map/ppermute | solution.py:80
  90.2 5.3 %collective-permute-start.5 = (bf16[512,128]{1,0:T(8,128)(2,1)S(1)}, bf16[512,128]{1,0:T(8,128)(2,1)S(1)}, u32[]{:S(2)}, u32[]{:S(2)}) collective-permute-start(bf16[512,128]{1,0:T(8,128)(2,1)S(1)} %collective-permute-done.4), channel_id=1, source_target_pairs={{0,1},{1,2},{2,3},{3,4},{4,5},{5,6},{6,7},{7,0},{8,9},{9,10},{10,1... | collective-permute-start | bytes 393224 | tf_op jit(solution)/shard_map/ppermute | solution.py:80
  95.5 5.3 %collective-permute-start.6 = (bf16[512,128]{1,0:T(8,128)(2,1)S(1)}, bf16[512,128]{1,0:T(8,128)(2,1)S(1)}, u32[]{:S(2)}, u32[]{:S(2)}) collective-permute-start(bf16[512,128]{1,0:T(8,128)(2,1)S(1)} %collective-permute-done.5), channel_id=1, source_target_pairs={{0,1},{1,2},{2,3},{3,4},{4,5},{5,6},{6,7},{7,0},{8,9},{9,10},{10,1... | collective-permute-start | bytes 393224 | tf_op jit(solution)/shard_map/ppermute | solution.py:80
  108.3 13.3 %all-to-all-start.4 = ((bf16[4,136,256]{2,1,0:T(8,128)(2,1)}), bf16[4,136,256]{2,1,0:T(8,128)(2,1)S(1)}, u32[]{:S(2)}, u32[]{:S(2)}) async-start(bf16[4,136,256]{2,1,0:T(8,128)(2,1)} %copy.85), calls=%async_computation.4 | async-start | bytes 557056 | tf_op jit(solution)/shard_map/all_to_all | solution.py:94
  113.4 40.7 %reduce-scatter.2.cloned.1.call-start = ((), (), s32[]{:S(2)}) async-start(), calls=%async_computation.10 | async-start | bytes 1179648 | tf_op jit(solution)/shard_map/reduce_scatter | solution.py:84
  119.4 6.9 %copy-start.5 = (bf16[544,1024]{0,1:T(8,128)(2,1)S(1)}, bf16[544,1024]{0,1:T(8,128)(2,1)}, u32[]{:S(2)}) copy-start(bf16[544,1024]{0,1:T(8,128)(2,1)} %all-gather.2.cloned.1.call-done) | copy-start | bytes 3342340
  121.5 11.4 %all-to-all-start.5 = ((bf16[4,136,256]{2,1,0:T(8,128)(2,1)}), bf16[4,136,256]{2,1,0:T(8,128)(2,1)S(1)}, u32[]{:S(2)}, u32[]{:S(2)}) async-start(bf16[4,136,256]{2,1,0:T(8,128)(2,1)} %copy.86), calls=%async_computation.5 | async-start | bytes 557056 | tf_op jit(solution)/shard_map/all_to_all | solution.py:95
  133.0 16.5 %all-to-all-start.6 = ((bf16[4,136,512]{2,1,0:T(8,128)(2,1)}), bf16[4,136,512]{2,1,0:T(8,128)(2,1)S(1)}, u32[]{:S(2)}, u32[]{:S(2)}) async-start(bf16[4,136,512]{2,1,0:T(8,128)(2,1)} %bitcast.11), calls=%async_computation.6 | async-start | bytes 1114112 | tf_op jit(solution)/shard_map/all_to_all | solution.py:100
  (2 other events, 8.1 us)
Sparse Core Ops, SparseCore 0:
  81.3 34.8 all-gather.1
  119.6 34.4 reduce-scatter.1
